TPU v7x, 512 devices: a whole 4x4x16 slice. The times are simulated.
512 devices in a mesh: fs: 64 (over z, y), tp: 8 (over x, core).
Axes of the slice: x: 4, y: 4, z: 16, core: 2. Of those that a mesh axis runs over, the one named last changes fastest.
Arguments:
- tokens: bfloat16 [16384, 2048], P('fs'), may hold values from -6 to 6
- recurrent_input_gain: bfloat16 [2048], replicated, may hold values from 0.099609375 to 1.8984375
- recurrent_branch_weight: bfloat16 [2048, 1024], P('fs', 'tp'), may hold values from -0.125 to 0.125
- output_gate_weight: bfloat16 [2048, 1024], P('fs', 'tp'), may hold values from -0.125 to 0.125
- filter_taps: bfloat16 [4, 1024], P(None, 'tp'), may hold values from -3 to 3
- retention_gate_blocks: bfloat16 [2, 8, 128, 128], P(None, 'tp'), may hold values from -0.5 to 0.5
- input_gate_blocks: bfloat16 [2, 8, 128, 128], P(None, 'tp'), may hold values from -0.5 to 0.5
- channel_decay_rate: float32 [2, 1024], P(None, 'tp'), may hold values from 0 to 0.008, as said below
- position_log_decay: float32 [2, 16384, 1024], P(None, 'fs', 'tp'), may hold values from -0.7 to 0, as said below
- recurrent_output_weight: bfloat16 [1024, 2048], P('tp', 'fs'), may hold values from -0.1875 to 0.1875
- recurrent_output_gain: bfloat16 [2048], replicated, may hold values from 0.099609375 to 1.8984375
- feedforward_norm_gain: bfloat16 [2048], replicated, may hold values from 0.099609375 to 1.8984375
- feedforward_up_weight: bfloat16 [2048, 8192], P('fs', 'tp'), may hold values from -0.125 to 0.125
- feedforward_down_weight: bfloat16 [8192, 2048], P('tp', 'fs'), may hold values from -0.0625 to 0.0625
- feedforward_output_gain: bfloat16 [2048], replicated, may hold values from 0.099609375 to 1.8984375
Outputs:
- layer_out: bfloat16 [16384, 2048], P('fs')
Inputs may be any that keep to these rules, and one draw needn't show every extreme that they name: `channel_decay_rate`: positive rates, one for each channel and direction. `position_log_decay`: zero except at a few positions of each sequence and channel.
All inputs are finite; a program needn't handle non-finite values.
Results may differ from a plain program's by a relative error of at most 0.02.
Values may be sent and summed in bfloat16 or wider, within the bound.
No kernel may reach another device: no remote copies, remote signals or barrier semaphores. Data moves between devices by JAX's collectives and lax.ppermute only.
A program may use at most 128 MiB of HBM per device.

v0:
```python
import jax
import jax.numpy as jnp
from jax import lax
from jax.sharding import Mesh
from jax.sharding import PartitionSpec as P

FS = ("zh", "zl", "y")
Z = ("zh", "zl")
TP = ("x", "c")
EPS = 1e-06
GATE_STEEPNESS = 8.0


def spread(array, axis):
    copies = jnp.broadcast_to(array, (lax.axis_size(axis), *array.shape))
    return lax.all_to_all(copies, axis, split_axis=0, concat_axis=0, tiled=True)


def mixer_weights(array):
    width = array.shape[-1]
    pieces = spread(spread(spread(array, "zh"), "zl"), "y")
    return jnp.transpose(pieces, (2, 1, 0, 3, 4)).reshape(-1, width)


def feedforward_weights(array):
    near = spread(array, "y").reshape(-1, array.shape[-1])
    return lax.all_gather(near, Z, axis=0, tiled=True)


def summed_rows(partial):
    cores, wide = (lax.axis_size("c"), lax.axis_size("x"))
    rows, width = partial.shape
    halves = partial.astype(jnp.bfloat16).reshape(cores, rows // cores, width)
    pair = lax.all_to_all(halves, "c", split_axis=0, concat_axis=0, tiled=True)
    half = jnp.sum(pair.astype(jnp.float32), axis=0).astype(jnp.bfloat16)
    quarters = half.reshape(wide, rows // (cores * wide), width)
    several = lax.all_to_all(quarters, "x", split_axis=0, concat_axis=0, tiled=True)
    return jnp.sum(several.astype(jnp.float32), axis=0)


def all_rows(part):
    return spread(spread(part, "x"), "c").reshape(-1, part.shape[-1])


def root_norm(values, gain):
    return (
        values
        * lax.rsqrt(jnp.mean(values * values, axis=-1, keepdims=True) + EPS)
        * gain.astype(jnp.float32)
    )


def combine(earlier, later):
    return (earlier[0] * later[0], later[0] * earlier[1] + later[1])


def centred_conv(signal, taps):
    length = signal.shape[0]
    width_taps = taps.shape[0]
    left_pad = width_taps // 2
    padded = jnp.pad(signal.astype(jnp.float32), ((left_pad, width_taps - 1 - left_pad), (0, 0)))
    total = jnp.zeros(signal.shape, jnp.float32)
    for offset in range(width_taps):
        total = total + padded[offset : offset + length] * taps[offset].astype(jnp.float32)
    return total.astype(jnp.bfloat16)


def block_map(signal, matrices):
    block_width = matrices.shape[-1]
    shaped = signal.reshape(signal.shape[0], matrices.shape[0], block_width)
    mapped = jnp.einsum("tnc,ncd->tnd", shaped, matrices, preferred_element_type=jnp.float32)
    return mapped.reshape(signal.shape)


def linear_recurrence(
    convolved_output,
    retention_matrices,
    input_gate_matrices,
    decay_rate_row,
    decay_extra_block,
    reversed_scan,
):
    retention_gate = jax.nn.sigmoid(block_map(convolved_output, retention_matrices))
    admit = jax.nn.sigmoid(block_map(convolved_output, input_gate_matrices))
    logarithm_decay = -GATE_STEEPNESS * retention_gate * decay_rate_row[None, :] + decay_extra_block
    decay = jnp.exp(logarithm_decay)
    drive = jnp.sqrt(-jnp.expm1(2.0 * logarithm_decay)) * (
        admit * convolved_output.astype(jnp.float32)
    )
    _, state = lax.associative_scan(combine, (decay, drive), reverse=reversed_scan, axis=0)
    return state


def per_device(
    tokens,
    recurrent_input_gain,
    recurrent_branch_weight,
    output_gate_weight,
    filter_taps,
    retention_gate_blocks,
    input_gate_blocks,
    channel_decay_rate,
    position_log_decay,
    recurrent_output_weight,
    recurrent_output_gain,
    feedforward_norm_gain,
    feedforward_up_weight,
    feedforward_down_weight,
    feedforward_output_gain,
):
    mixer = mixer_weights(
        jnp.concatenate(
            (recurrent_branch_weight, output_gate_weight, recurrent_output_weight.T), axis=1
        )
    )
    forward = feedforward_weights(
        jnp.concatenate((feedforward_up_weight, feedforward_down_weight.T), axis=1)
    )
    channels = recurrent_branch_weight.shape[1]
    hidden_units = feedforward_up_weight.shape[1]
    normed = root_norm(tokens.astype(jnp.float32), recurrent_input_gain).astype(jnp.bfloat16)
    recur_sum = jnp.dot(normed, mixer[:, :channels], preferred_element_type=jnp.float32)
    gate_sum = jnp.dot(
        normed, mixer[:, channels : 2 * channels], preferred_element_type=jnp.float32
    )
    recur_in = recur_sum.astype(jnp.bfloat16)
    gate_in = lax.optimization_barrier(gate_sum.astype(jnp.bfloat16))
    convolved_output = lax.optimization_barrier(centred_conv(recur_in, filter_taps))
    forward_sweep = linear_recurrence(
        convolved_output,
        retention_gate_blocks[0],
        input_gate_blocks[0],
        channel_decay_rate[0],
        position_log_decay[0],
        False,
    )
    backward_sweep = linear_recurrence(
        convolved_output,
        retention_gate_blocks[1],
        input_gate_blocks[1],
        channel_decay_rate[1],
        position_log_decay[1],
        True,
    )
    hidden = ((forward_sweep + backward_sweep) * jax.nn.gelu(gate_in.astype(jnp.float32))).astype(
        jnp.bfloat16
    )
    across = (((1,), (1,)), ((), ()))
    partial_value = lax.dot_general(
        hidden, mixer[:, 2 * channels :], across, preferred_element_type=jnp.float32
    )
    mixed = summed_rows(partial_value)
    share = mixed.shape[0]
    place = lax.axis_index("c") * lax.axis_size("x") + lax.axis_index("x")
    own = lax.dynamic_slice_in_dim(tokens, place * share, share, axis=0)
    stream = lax.optimization_barrier(
        (own.astype(jnp.float32) + root_norm(mixed, recurrent_output_gain)).astype(jnp.bfloat16)
    )
    normed_ff = all_rows(
        root_norm(stream.astype(jnp.float32), feedforward_norm_gain).astype(jnp.bfloat16)
    )
    lifted_sum = jnp.dot(normed_ff, forward[:, :hidden_units], preferred_element_type=jnp.float32)
    lifted = jnp.square(jax.nn.relu(lifted_sum)).astype(jnp.bfloat16)
    lowered_part = lax.dot_general(
        lifted, forward[:, hidden_units:], across, preferred_element_type=jnp.float32
    )
    lowered = summed_rows(lowered_part)
    return all_rows(
        (stream.astype(jnp.float32) + root_norm(lowered, feedforward_output_gain)).astype(
            jnp.bfloat16
        )
    )


def solution(mesh):
    split = Mesh(mesh.devices.reshape(4, 4, 4, 4, 2), ("zh", "zl", "y", "x", "c"))
    placed = (
        P(FS, None),
        P(),
        P(FS, TP),
        P(FS, TP),
        P(None, TP),
        P(None, TP, None, None),
        P(None, TP, None, None),
        P(None, TP),
        P(None, FS, TP),
        P(TP, FS),
        P(),
        P(),
        P(FS, TP),
        P(TP, FS),
        P(),
    )
    return jax.shard_map(
        per_device, mesh=split, in_specs=placed, out_specs=P(FS, None), check_vma=False
    )
```

profile of v0, /device:TPU:1, one launch (start us, length us, event | category | flops | bytes accessed | tf_op | source)
XLA Modules:
  0.0 197.8 jit_solution(3775342261377524410)
XLA Ops:
  6.5 0.9 pad_maximum_fusion
  7.4 0.8 broadcast_in_dim.41
  8.3 5.0 %all-to-all-start.7 = ((bf16[4,32,2048]{2,1,0:T(8,128)(2,1)}), bf16[4,32,2048]{2,1,0:T(8,128)(2,1)S(1)}, u32[]{:S(2)}, u32[]{:S(2)}) async-start(bf16[4,32,2048]{2,1,0:T(8,128)(2,1)} %broadcast_in_dim.41), calls=%async_computation.7 | async-start | bytes 1048576 | tf_op jit(solution)/shard_map/all_to_all | solution.py:16
  13.3 0.7 pad_maximum_fusion.5
  14.0 6.2 %all-to-all-done.7 = bf16[4,32,2048]{2,1,0:T(8,128)(2,1)S(1)} async-done(((bf16[4,32,2048]{2,1,0:T(8,128)(2,1)}), bf16[4,32,2048]{2,1,0:T(8,128)(2,1)S(1)}, u32[]{:S(2)}, u32[]{:S(2)}) %all-to-all-start.7) | async-done | bytes 524320 | tf_op jit(solution)/shard_map/all_to_all | solution.py:16
  20.2 0.7 broadcast_in_dim.16
  20.9 16.2 %all-to-all-start = ((bf16[4,32,384]{2,1,0:T(8,128)(2,1)}), bf16[4,32,384]{2,1,0:T(8,128)(2,1)S(1)}, u32[]{:S(2)}, u32[]{:S(2)}) async-start(bf16[4,32,384]{2,1,0:T(8,128)(2,1)} %broadcast_in_dim.16), calls=%async_computation | async-start | bytes 196608 | tf_op jit(solution)/shard_map/all_to_all | solution.py:16
  37.1 0.0 all-gather.2.cloned.1.call-start
  37.1 0.0 copy-done
  37.1 0.7 all-gather.2.cloned.1.call-update
  37.8 11.2 %all-to-all-done = bf16[4,32,384]{2,1,0:T(8,128)(2,1)S(1)} async-done(((bf16[4,32,384]{2,1,0:T(8,128)(2,1)}), bf16[4,32,384]{2,1,0:T(8,128)(2,1)S(1)}, u32[]{:S(2)}, u32[]{:S(2)}) %all-to-all-start) | async-done | bytes 98336 | tf_op jit(solution)/shard_map/all_to_all | solution.py:16
  49.0 10.6 %all_to_all.60 = bf16[4,4,32,384]{3,2,1,0:T(8,128)(2,1)S(1)} all-to-all(bf16[4,4,32,384]{3,2,1,0:T(8,128)(2,1)S(1)} %broadcast_in_dim.17), channel_id=1, replica_groups=mesh['zh'=4,'zl'=4,'y'=4,'x'=4,'c'=2] {'zl'}, dimensions={0} | all-to-all | bytes 786432 | tf_op jit(solution)/shard_map/all_to_all | solution.py:16
  59.6 0.0 copy-start.4
  59.6 1.4 broadcast_in_dim.18
  61.1 3.7 %all-to-all-start.2 = ((bf16[4,4,4,32,384]{4,3,1,2,0:T(8,128)(2,1)}), bf16[4,4,4,32,384]{4,3,1,2,0:T(8,128)(2,1)S(1)}, u32[]{:S(2)}, u32[]{:S(2)}) async-start(bf16[4,4,4,32,384]{4,3,1,2,0:T(8,128)(2,1)} %broadcast_in_dim.18), calls=%async_computation.2 | async-start | bytes 3145728 | tf_op jit(solution)/shard_map/all_to_all | solution.py:16
  64.8 0.0 copy-done.1
  64.8 0.3 fusion.7
  65.1 12.2 %all-to-all-done.2 = bf16[4,4,4,32,384]{4,3,1,2,0:T(8,128)(2,1)S(1)} async-done(((bf16[4,4,4,32,384]{4,3,1,2,0:T(8,128)(2,1)}), bf16[4,4,4,32,384]{4,3,1,2,0:T(8,128)(2,1)S(1)}, u32[]{:S(2)}, u32[]{:S(2)}) %all-to-all-start.2) | async-done | bytes 1572896 | tf_op jit(solution)/shard_map/all_to_all | solution.py:16
  77.3 0.2 copy.19
  77.6 0.0 copy-start.10
  77.6 0.0 copy-start.11
  77.6 0.0 copy-start.12
  77.6 1.8 fusion.41
  79.4 0.1 add_convert_fusion.1
  79.5 0.2 fusion.102
  79.7 0.0 copy-done.12
  79.7 0.2 fusion.32
  79.9 0.0 copy-start.3
  80.8 0.2 fusion.103
  81.0 0.2 fusion.40
  81.3 0.0 slice-start
  82.5 0.0 copy-start.2
  83.3 0.1 rev.2
  83.4 0.4 copy-done.2
  83.8 0.5 convolution_convert_fusion.1
  84.3 0.4 convolution_convert_fusion
  84.7 0.0 copy-start.5
  84.7 0.0 copy-start.6
  84.7 14.9 %all_to_all.61 = bf16[2,128,2048]{2,1,0:T(8,128)(2,1)S(1)} all-to-all(bf16[2,128,2048]{2,1,0:T(8,128)(2,1)S(1)} %bitcast.53), channel_id=1, replica_groups=mesh['zh'=4,'zl'=4,'y'=4,'x'=4,'c'=2] {'c'}, dimensions={0} | all-to-all | bytes 2097152 | tf_op jit(solution)/shard_map/all_to_all | solution.py:34
  99.7 1.1 reduce_sum.79
  100.8 4.0 %all-to-all-start.4 = ((bf16[4,32,2048]{2,1,0:T(8,128)(2,1)}), bf16[4,32,2048]{2,1,0:T(8,128)(2,1)S(1)}, u32[]{:S(2)}, u32[]{:S(2)}) async-start(bf16[4,32,2048]{2,1,0:T(8,128)(2,1)} %bitcast.17), calls=%async_computation.4 | async-start | bytes 1048576 | tf_op jit(solution)/shard_map/all_to_all | solution.py:37
  104.8 8.9 %all-to-all-done.4 = bf16[4,32,2048]{2,1,0:T(8,128)(2,1)S(1)} async-done(((bf16[4,32,2048]{2,1,0:T(8,128)(2,1)}), bf16[4,32,2048]{2,1,0:T(8,128)(2,1)S(1)}, u32[]{:S(2)}, u32[]{:S(2)}) %all-to-all-start.4) | async-done | bytes 524320 | tf_op jit(solution)/shard_map/all_to_all | solution.py:37
  113.7 0.1 convert_reduce_fusion.1
  113.8 0.1 multiply_reduce_fusion.1
  113.9 0.1 add_convert_fusion
  114.0 0.1 fusion.48
  114.2 0.1 fusion.50
  114.3 10.2 %all_to_all.62 = bf16[4,32,2048]{2,1,0:T(8,128)(2,1)S(1)} all-to-all(bf16[4,32,2048]{2,1,0:T(8,128)(2,1)S(1)} %broadcast_in_dim.19), channel_id=1, replica_groups=mesh['zh'=4,'zl'=4,'y'=4,'x'=4,'c'=2] {'x'}, dimensions={0} | all-to-all | bytes 1048576 | tf_op jit(solution)/shard_map/all_to_all | solution.py:16
  124.6 0.1 broadcast_in_dim.40
  124.7 6.8 %all_to_all.63 = bf16[2,4,32,2048]{3,2,1,0:T(8,128)(2,1)S(1)} all-to-all(bf16[2,4,32,2048]{3,2,1,0:T(8,128)(2,1)S(1)} %broadcast_in_dim.40), channel_id=1, replica_groups=mesh['zh'=4,'zl'=4,'y'=4,'x'=4,'c'=2] {'c'}, dimensions={0} | all-to-all | bytes 2097152 | tf_op jit(solution)/shard_map/all_to_all | solution.py:16
  131.5 16.2 %all-gather.2.cloned.1.call-done = bf16[2048,2048]{1,0:T(8,128)(2,1)} async-done(((bf16[128,2048]{1,0:T(8,128)(2,1)}), bf16[2048,2048]{1,0:T(8,128)(2,1)}) %all-gather.2.cloned.1.call-update) | async-done | bytes 8388624 | tf_op jit(solution)/shard_map/all_gather | solution.py:27
  147.7 5.8 %fusion.4 = bf16[256,2048]{1,0:T(8,128)(2,1)S(1)} fusion(bf16[2048,2048]{1,0:T(8,128)(2,1)} %all-gather.2.cloned.1.call-done, bf16[256,2048]{1,0:T(8,128)(2,1)S(1)} %bitcast.59), kind=kOutput, calls=%fused_computation.7 | convolution fusion | flops 2148794368 | bytes 10485760 | tf_op jit(solution)/shard_map/dot_general | solution.py:164
  153.5 0.0 copy-start.7
  153.5 5.0 %all_to_all.64 = bf16[2,128,2048]{2,1,0:T(8,128)(2,1)S(1)} all-to-all(bf16[2,128,2048]{2,1,0:T(8,128)(2,1)S(1)} %bitcast.60), channel_id=1, replica_groups=mesh['zh'=4,'zl'=4,'y'=4,'x'=4,'c'=2] {'c'}, dimensions={0} | all-to-all | bytes 2097152 | tf_op jit(solution)/shard_map/all_to_all | solution.py:34
  158.5 1.1 reduce_sum.83
  159.6 4.0 %all-to-all-start.9 = ((bf16[4,32,2048]{2,1,0:T(8,128)(2,1)}), bf16[4,32,2048]{2,1,0:T(8,128)(2,1)S(1)}, u32[]{:S(2)}, u32[]{:S(2)}) async-start(bf16[4,32,2048]{2,1,0:T(8,128)(2,1)} %bitcast.22), calls=%async_computation.9 | async-start | bytes 1048576 | tf_op jit(solution)/shard_map/all_to_all | solution.py:37
  163.5 8.9 %all-to-all-done.9 = bf16[4,32,2048]{2,1,0:T(8,128)(2,1)S(1)} async-done(((bf16[4,32,2048]{2,1,0:T(8,128)(2,1)}), bf16[4,32,2048]{2,1,0:T(8,128)(2,1)S(1)}, u32[]{:S(2)}, u32[]{:S(2)}) %all-to-all-start.9) | async-done | bytes 524320 | tf_op jit(solution)/shard_map/all_to_all | solution.py:37
  172.5 0.1 convert_reduce_fusion
  172.5 0.1 multiply_reduce_fusion
  172.7 0.1 fusion.51
  172.8 10.2 %all_to_all.65 = bf16[4,32,2048]{2,1,0:T(8,128)(2,1)S(1)} all-to-all(bf16[4,32,2048]{2,1,0:T(8,128)(2,1)S(1)} %broadcast_in_dim.42), channel_id=1, replica_groups=mesh['zh'=4,'zl'=4,'y'=4,'x'=4,'c'=2] {'x'}, dimensions={0} | all-to-all | bytes 1048576 | tf_op jit(solution)/shard_map/all_to_all | solution.py:16
  183.0 0.1 broadcast_in_dim.43
  183.2 6.8 %all_to_all.66 = bf16[2,4,32,2048]{3,2,1,0:T(8,128)(2,1)S(1)} all-to-all(bf16[2,4,32,2048]{3,2,1,0:T(8,128)(2,1)S(1)} %broadcast_in_dim.43), channel_id=1, replica_groups=mesh['zh'=4,'zl'=4,'y'=4,'x'=4,'c'=2] {'c'}, dimensions={0} | all-to-all | bytes 2097152 | tf_op jit(solution)/shard_map/all_to_all | solution.py:16
  190.0 1.0 copy.21
  (212 shorter events, 2.4 us)
Async XLA Ops:
  8.3 11.9 %all-to-all-start.7 = ((bf16[4,32,2048]{2,1,0:T(8,128)(2,1)}), bf16[4,32,2048]{2,1,0:T(8,128)(2,1)S(1)}, u32[]{:S(2)}, u32[]{:S(2)}) async-start(bf16[4,32,2048]{2,1,0:T(8,128)(2,1)} %broadcast_in_dim.41), calls=%async_computation.7 | async-start | bytes 1048576 | tf_op jit(solution)/shard_map/all_to_all | solution.py:16
  20.2 16.9 %copy-start = (bf16[4,32,2048]{2,1,0:T(8,128)(2,1)}, bf16[4,32,2048]{2,1,0:T(8,128)(2,1)S(1)}, u32[]{:S(2)}) copy-start(bf16[4,32,2048]{2,1,0:T(8,128)(2,1)S(1)} %all-to-all-done.7) | copy-start | bytes 1572868
  20.9 28.1 %all-to-all-start = ((bf16[4,32,384]{2,1,0:T(8,128)(2,1)}), bf16[4,32,384]{2,1,0:T(8,128)(2,1)S(1)}, u32[]{:S(2)}, u32[]{:S(2)}) async-start(bf16[4,32,384]{2,1,0:T(8,128)(2,1)} %broadcast_in_dim.16), calls=%async_computation | async-start | bytes 196608 | tf_op jit(solution)/shard_map/all_to_all | solution.py:16
  37.1 110.6 %all-gather.2.cloned.1.call-start = ((), (), s32[]{:S(2)}) async-start(), calls=%async_computation.12 | async-start | bytes 8912896 | tf_op jit(solution)/shard_map/all_gather | solution.py:27
  59.6 5.1 %copy-start.4 = (bf16[2048]{0:T(1024)(128)(2,1)S(1)}, bf16[2048]{0:T(1024)(128)(2,1)}, u32[]{:S(2)}) copy-start(bf16[2048]{0:T(1024)(128)(2,1)} %param.16) | copy-start | bytes 12292
  61.0 3.7 %copy-start.1 = (bf16[256,2048]{1,0:T(8,128)(2,1)S(1)}, bf16[256,2048]{1,0:T(8,128)(2,1)}, u32[]{:S(2)}) copy-start(bf16[256,2048]{1,0:T(8,128)(2,1)} %param.15) | copy-start | bytes 3145732
  61.0 4.0 %copy-start.9 = (f32[2,128]{1,0:T(2,128)S(1)}, f32[2,128]{1,0:T(2,128)}, u32[]{:S(2)}) copy-start(f32[2,128]{1,0:T(2,128)} %param.22) | copy-start | bytes 3076
  61.0 4.1 %copy-start.8 = (bf16[4,128]{1,0:T(4,128)(2,1)S(1)}, bf16[4,128]{1,0:T(4,128)(2,1)}, u32[]{:S(2)}) copy-start(bf16[4,128]{1,0:T(4,128)(2,1)} %param.19) | copy-start | bytes 3076
  61.1 16.3 %all-to-all-start.2 = ((bf16[4,4,4,32,384]{4,3,1,2,0:T(8,128)(2,1)}), bf16[4,4,4,32,384]{4,3,1,2,0:T(8,128)(2,1)S(1)}, u32[]{:S(2)}, u32[]{:S(2)}) async-start(bf16[4,4,4,32,384]{4,3,1,2,0:T(8,128)(2,1)} %broadcast_in_dim.18), calls=%async_computation.2 | async-start | bytes 3145728 | tf_op jit(solution)/shard_map/all_to_all | solution.py:16
  77.6 1.9 copy-start.10
  77.6 1.9 copy-start.11
  77.6 2.1 %copy-start.12 = (bf16[2,1,128,128]{3,2,1,0:T(8,128)(2,1)S(1)}, bf16[2,1,128,128]{3,2,1,0:T(8,128)(2,1)}, u32[]{:S(2)}) copy-start(bf16[2,1,128,128]{3,2,1,0:T(8,128)(2,1)} %param.21) | copy-start | bytes 196612
  79.9 1.3 copy-start.3
  81.3 1.4 slice-start
  82.5 1.2 copy-start.2
  84.7 20.0 %copy-start.5 = (bf16[2048]{0:T(1024)(128)(2,1)S(1)}, bf16[2048]{0:T(1024)(128)(2,1)}, u32[]{:S(2)}) copy-start(bf16[2048]{0:T(1024)(128)(2,1)} %param.25) | copy-start | bytes 12292
  84.7 20.0 %copy-start.6 = (bf16[2048]{0:T(1024)(128)(2,1)S(1)}, bf16[2048]{0:T(1024)(128)(2,1)}, u32[]{:S(2)}) copy-start(bf16[2048]{0:T(1024)(128)(2,1)} %param.26) | copy-start | bytes 12292
  100.8 12.9 %all-to-all-start.4 = ((bf16[4,32,2048]{2,1,0:T(8,128)(2,1)}), bf16[4,32,2048]{2,1,0:T(8,128)(2,1)S(1)}, u32[]{:S(2)}, u32[]{:S(2)}) async-start(bf16[4,32,2048]{2,1,0:T(8,128)(2,1)} %bitcast.17), calls=%async_computation.4 | async-start | bytes 1048576 | tf_op jit(solution)/shard_map/all_to_all | solution.py:37
  153.5 10.1 %copy-start.7 = (bf16[2048]{0:T(1024)(128)(2,1)S(1)}, bf16[2048]{0:T(1024)(128)(2,1)}, u32[]{:S(2)}) copy-start(bf16[2048]{0:T(1024)(128)(2,1)} %param.29) | copy-start | bytes 12292
  159.6 12.9 %all-to-all-start.9 = ((bf16[4,32,2048]{2,1,0:T(8,128)(2,1)}), bf16[4,32,2048]{2,1,0:T(8,128)(2,1)S(1)}, u32[]{:S(2)}, u32[]{:S(2)}) async-start(bf16[4,32,2048]{2,1,0:T(8,128)(2,1)} %bitcast.22), calls=%async_computation.9 | async-start | bytes 1048576 | tf_op jit(solution)/shard_map/all_to_all | solution.py:37
Sparse Core Ops, SparseCore 0:
  40.0 107.6 all-gather.1
where the time goes:
time: 199 us; the launch traced here: 198 us
  blocking collectives  64.5 us (32%)
  waiting for transfers between devices  64.2 us (32%)
  starting transfers between devices  32.8 us (16%)
  between operations  14.6 us (7%)
  matrix products  9.29 us (5%)
  local copies, waits for them, and re-layouts  6.69 us (3%)
  other arithmetic  5.67 us (3%)
    all_to_all x5, blocking collectives, spread(): return lax.all_to_all(copies, axis, split_axis=0, concat_axis=0, tiled=True)  44.6 us
    all_to_all x3, waiting for transfers between devices, spread(): return lax.all_to_all(copies, axis, split_axis=0, concat_axis=0, tiled=True)  29.5 us
    all_to_all x3, starting transfers between devices, spread(): return lax.all_to_all(copies, axis, split_axis=0, concat_axis=0, tiled=True)  24.9 us
    all_to_all x2, blocking collectives, summed_rows(): pair = lax.all_to_all(halves, 'c', split_axis=0, concat_axis=0, tiled=True)  19.9 us
    all_to_all x2, waiting for transfers between devices, summed_rows(): lax.all_to_all(quarters, 'x', split_axis=0, concat_axis=0, tiled=True)  17.8 us
    all_gather x1, waiting for transfers between devices, feedforward_weights(): return lax.all_gather(near, Z, axis=0, tiled=True)  16.2 us
    all_to_all x2, starting transfers between devices, summed_rows(): lax.all_to_all(quarters, 'x', split_axis=0, concat_axis=0, tiled=True)  7.93 us
    dot_general x1, matrix products, per_device(): lax.dot_general(lifted, forward[:, hidden_units:], across, preferred_elem...  5.81 us
  transfers between devices with their start and end apart: 6, of which 6 were waited for; matrix products, arithmetic and copies ran while one was open for 5% of the time, Pallas kernels for 0%

commit v1 on v0

--- a/solution.py
+++ b/solution.py
@@ -11,6 +11,13 @@
 GATE_STEEPNESS = 8.0
 
 
+def gather_over(shard, axis, along):
+    n_dev = lax.axis_size(axis)
+    tiles = jnp.stack([shard for _ in range(n_dev)])
+    tiles = lax.all_to_all(tiles, axis, split_axis=0, concat_axis=0)
+    return jnp.concatenate(tiles, axis=along)
+
+
 def spread(array, axis):
     copies = jnp.broadcast_to(array, (lax.axis_size(axis), *array.shape))
     return lax.all_to_all(copies, axis, split_axis=0, concat_axis=0, tiled=True)
@@ -24,7 +31,7 @@
 
 def feedforward_weights(array):
     near = spread(array, "y").reshape(-1, array.shape[-1])
-    return lax.all_gather(near, Z, axis=0, tiled=True)
+    return gather_over(near, Z, 0)
 
 
 def summed_rows(partial):

time: 199 us -> 566 us (2.84)
  blocking collectives: 64.5 us -> 462 us
  waiting for transfers between devices: 64.2 us -> 40.4 us
  starting transfers between devices: 32.8 us -> 15.3 us
  between operations: 14.6 us -> 1.01 us
  local copies, waits for them, and re-layouts: 6.69 us -> 18.1 us
  other arithmetic: 5.67 us -> 13.4 us
    all_to_all x0 -> x1, blocking collectives: none -> 366 us  [gather_over(): tiles = lax.all_to_all(tiles, axis, split_axis=0, concat_axis=0)]
    all_to_all x5 -> x6, blocking collectives: 44.6 us -> 73.7 us  [spread(): return lax.all_to_all(copies, axis, split_axis=0, concat_axis=0, tiled=True)]
    all_to_all x3 -> x2, starting transfers between devices: 24.9 us -> 7.79 us  [spread(): return lax.all_to_all(copies, axis, split_axis=0, concat_axis=0, tiled=True)]
    all_gather x1 -> x0, waiting for transfers between devices: 16.2 us -> none  [feedforward_weights(): return lax.all_gather(near, Z, axis=0, tiled=True)]
    slice x99 -> x98, local copies, waits for them, and re-layouts: 1.37 us -> 12.5 us  [linear_recurrence(): lax.associative_scan(combine, (decay, drive), reverse=reversed_scan, axis=0)]
    all_to_all x3 -> x2, waiting for transfers between devices: 29.5 us -> 22.4 us  [spread(): return lax.all_to_all(copies, axis, split_axis=0, concat_axis=0, tiled=True)]
  transfers between devices with their start and end apart: 6 -> 4, of which waited for: 6 -> 4; matrix products, arithmetic and copies ran while one was open for 5% -> 0% of each run, Pallas kernels for 0% -> 0%
where the time goes in v1:
time: 566 us; the launch traced here: 565 us
  blocking collectives  462 us (82%)
  waiting for transfers between devices  40.4 us (7%)
  local copies, waits for them, and re-layouts  18.1 us (3%)
  starting transfers between devices  15.3 us (3%)
  matrix products  14.3 us (3%)
  other arithmetic  13.4 us (2%)
    all_to_all x1, blocking collectives, gather_over(): tiles = lax.all_to_all(tiles, axis, split_axis=0, concat_axis=0)  366 us
    all_to_all x6, blocking collectives, spread(): return lax.all_to_all(copies, axis, split_axis=0, concat_axis=0, tiled=True)  73.7 us
    all_to_all x2, blocking collectives, summed_rows(): pair = lax.all_to_all(halves, 'c', split_axis=0, concat_axis=0, tiled=True)  22.6 us
    all_to_all x2, waiting for transfers between devices, spread(): return lax.all_to_all(copies, axis, split_axis=0, concat_axis=0, tiled=True)  22.4 us
    all_to_all x2, waiting for transfers between devices, summed_rows(): lax.all_to_all(quarters, 'x', split_axis=0, concat_axis=0, tiled=True)  18 us
    slice x98, local copies, waits for them, and re-layouts, linear_recurrence(): lax.associative_scan(combine, (decay, drive), reverse=reversed_scan, axis=0)  12.5 us
  transfers between devices with their start and end apart: 4, of which 4 were waited for; matrix products, arithmetic and copies ran while one was open for 0% of the time, Pallas kernels for 0%

profile of v1, /device:TPU:1, one launch (start us, length us, event | category | flops | bytes accessed | tf_op | source)
XLA Modules:
  0.0 564.7 jit_solution(11586163537278222041)
XLA Ops:
  0.0 0.7 pad_maximum_fusion.5
  0.7 28.0 %all_to_all.65 = bf16[4,32,384]{2,1,0:T(8,128)(2,1)S(1)} all-to-all(bf16[4,32,384]{2,1,0:T(8,128)(2,1)S(1)} %broadcast_in_dim.16), channel_id=1, replica_groups=mesh['zh'=4,'zl'=4,'y'=4,'x'=4,'c'=2] {'zh'}, dimensions={0} | all-to-all | bytes 196608 | tf_op jit(solution)/shard_map/all_to_all | solution.py:23
  28.8 11.3 %all_to_all.66 = bf16[4,4,32,384]{3,2,1,0:T(8,128)(2,1)S(1)} all-to-all(bf16[4,4,32,384]{3,2,1,0:T(8,128)(2,1)S(1)} %broadcast_in_dim.17), channel_id=1, replica_groups=mesh['zh'=4,'zl'=4,'y'=4,'x'=4,'c'=2] {'zl'}, dimensions={0} | all-to-all | bytes 786432 | tf_op jit(solution)/shard_map/all_to_all | solution.py:23
  40.2 1.4 broadcast_in_dim.18
  41.5 4.3 all-to-all-start.2
  46.2 0.6 multiply_bitcast_fusion.1
  46.8 15.3 %all-to-all-done.2 = bf16[4,4,4,32,384]{4,3,1,2,0:T(8,128)(2,1)S(1)} async-done(((bf16[4,4,4,32,384]{4,3,1,2,0:T(8,128)(2,1)}), bf16[4,4,4,32,384]{4,3,1,2,0:T(8,128)(2,1)S(1)}, u32[]{:S(2)}, u32[]{:S(2)}) %all-to-all-start.2) | async-done | bytes 1572896 | tf_op jit(solution)/shard_map/all_to_all | solution.py:23
  62.3 1.8 convolution_convert_fusion.1
  64.2 0.5 fusion.41
  65.1 0.9 fusion.103
  66.0 1.1 fusion.40
  67.4 0.6 slice.580
  68.1 0.6 slice.551
  68.7 0.6 slice.576
  69.3 0.6 slice.557
  70.0 0.6 slice.574
  70.6 0.6 slice.568
  71.2 0.6 slice.564
  71.8 0.6 slice.566
  72.4 0.6 slice.565
  73.0 0.5 slice.555
  73.5 0.6 slice.608
  74.1 0.6 slice.578
  74.7 0.6 slice.545
  75.3 0.5 slice.607
  75.8 0.6 slice.606
  76.4 0.5 slice.605
  76.9 0.5 slice.604
  77.4 1.8 fusion.102
  79.3 1.1 fusion.32
  81.1 0.7 fusion.101
  81.8 0.8 fusion.98
  82.6 0.5 slice.487
  83.1 0.6 slice.595
  83.8 0.5 slice.594
  84.5 0.7 multiply_add_fusion.12
  85.1 0.6 pad_maximum_fusion.13
  85.8 0.7 multiply_add_fusion.8
  86.5 0.7 pad_maximum_fusion.11
  87.2 0.7 fusion.79
  87.9 0.6 pad_maximum_fusion.9
  88.5 0.7 fusion.77
  89.3 0.7 pad_maximum_fusion.7
  90.0 0.6 pad_maximum_fusion.4
  90.7 0.6 pad_maximum_fusion.2
  92.5 9.8 %all_to_all.67 = bf16[2,128,2048]{2,1,0:T(8,128)(2,1)S(1)} all-to-all(bf16[2,128,2048]{2,1,0:T(8,128)(2,1)S(1)} %bitcast.55), channel_id=1, replica_groups=mesh['zh'=4,'zl'=4,'y'=4,'x'=4,'c'=2] {'c'}, dimensions={0} | all-to-all | bytes 2097152 | tf_op jit(solution)/shard_map/all_to_all | solution.py:41
  102.3 1.1 reduce_sum.79
  103.4 4.0 all-to-all-start.4
  107.5 8.9 %all-to-all-done.4 = bf16[4,32,2048]{2,1,0:T(8,128)(2,1)S(1)} async-done(((bf16[4,32,2048]{2,1,0:T(8,128)(2,1)}), bf16[4,32,2048]{2,1,0:T(8,128)(2,1)S(1)}, u32[]{:S(2)}, u32[]{:S(2)}) %all-to-all-start.4) | async-done | bytes 524320 | tf_op jit(solution)/shard_map/all_to_all | solution.py:44
  116.3 0.8 broadcast_in_dim.41
  117.2 3.5 all-to-all-start.7
  121.3 7.1 %all-to-all-done.7 = bf16[4,32,2048]{2,1,0:T(8,128)(2,1)S(1)} async-done(((bf16[4,32,2048]{2,1,0:T(8,128)(2,1)}), bf16[4,32,2048]{2,1,0:T(8,128)(2,1)S(1)}, u32[]{:S(2)}, u32[]{:S(2)}) %all-to-all-start.7) | async-done | bytes 524320 | tf_op jit(solution)/shard_map/all_to_all | solution.py:23
  128.4 9.3 %all_to_all.68 = bf16[4,32,2048]{2,1,0:T(8,128)(2,1)S(1)} all-to-all(bf16[4,32,2048]{2,1,0:T(8,128)(2,1)S(1)} %broadcast_in_dim.19), channel_id=1, replica_groups=mesh['zh'=4,'zl'=4,'y'=4,'x'=4,'c'=2] {'x'}, dimensions={0} | all-to-all | bytes 1048576 | tf_op jit(solution)/shard_map/all_to_all | solution.py:23
  137.9 8.0 %all_to_all.69 = bf16[2,4,32,2048]{3,2,1,0:T(8,128)(2,1)S(1)} all-to-all(bf16[2,4,32,2048]{3,2,1,0:T(8,128)(2,1)S(1)} %broadcast_in_dim.40), channel_id=1, replica_groups=mesh['zh'=4,'zl'=4,'y'=4,'x'=4,'c'=2] {'c'}, dimensions={0} | all-to-all | bytes 2097152 | tf_op jit(solution)/shard_map/all_to_all | solution.py:23
  145.9 1.0 stack.3
  147.0 365.9 %all_to_all.70 = bf16[16,128,2048]{2,1,0:T(8,128)(2,1)} all-to-all(bf16[16,128,2048]{2,1,0:T(8,128)(2,1)S(1)} %stack.3), channel_id=1, replica_groups=mesh['zh'=4,'zl'=4,'y'=4,'x'=4,'c'=2] {'zh','zl'}, dimensions={0} | all-to-all | bytes 16777216 | tf_op jit(solution)/shard_map/all_to_all | solution.py:17
  512.9 6.8 %fusion.4 = bf16[256,2048]{1,0:T(8,128)(2,1)} fusion(bf16[2048,2048]{1,0:T(8,128)(2,1)} %bitcast.54, bf16[256,2048]{1,0:T(8,128)(2,1)S(1)} %bitcast.61), kind=kOutput, calls=%fused_computation.7 | convolution fusion | flops 2148794368 | bytes 10485760 | tf_op jit(solution)/shard_map/dot_general | solution.py:171
  519.7 12.7 %all_to_all.71 = bf16[2,128,2048]{2,1,0:T(8,128)(2,1)S(1)} all-to-all(bf16[2,128,2048]{2,1,0:T(8,128)(2,1)} %bitcast.62), channel_id=1, replica_groups=mesh['zh'=4,'zl'=4,'y'=4,'x'=4,'c'=2] {'c'}, dimensions={0} | all-to-all | bytes 2097152 | tf_op jit(solution)/shard_map/all_to_all | solution.py:41
  532.4 1.1 reduce_sum.83
  533.5 3.5 all-to-all-start.10
  537.0 9.1 %all-to-all-done.10 = bf16[4,32,2048]{2,1,0:T(8,128)(2,1)S(1)} async-done(((bf16[4,32,2048]{2,1,0:T(8,128)(2,1)}), bf16[4,32,2048]{2,1,0:T(8,128)(2,1)S(1)}, u32[]{:S(2)}, u32[]{:S(2)}) %all-to-all-start.10) | async-done | bytes 524320 | tf_op jit(solution)/shard_map/all_to_all | solution.py:44
  546.5 10.7 %all_to_all.72 = bf16[4,32,2048]{2,1,0:T(8,128)(2,1)S(1)} all-to-all(bf16[4,32,2048]{2,1,0:T(8,128)(2,1)S(1)} %broadcast_in_dim.42), channel_id=1, replica_groups=mesh['zh'=4,'zl'=4,'y'=4,'x'=4,'c'=2] {'x'}, dimensions={0} | all-to-all | bytes 1048576 | tf_op jit(solution)/shard_map/all_to_all | solution.py:23
  557.4 6.3 %all_to_all.73 = bf16[2,4,32,2048]{3,2,1,0:T(8,128)(2,1)S(1)} all-to-all(bf16[2,4,32,2048]{3,2,1,0:T(8,128)(2,1)S(1)} %broadcast_in_dim.43), channel_id=1, replica_groups=mesh['zh'=4,'zl'=4,'y'=4,'x'=4,'c'=2] {'c'}, dimensions={0} | all-to-all | bytes 2097152 | tf_op jit(solution)/shard_map/all_to_all | solution.py:23
  563.7 1.0 copy.21
  (219 shorter events, 4.7 us)
Async XLA Ops:
  40.2 5.7 %copy-start.6 = (bf16[2048]{0:T(1024)(128)(2,1)S(1)}, bf16[2048]{0:T(1024)(128)(2,1)}, u32[]{:S(2)}) copy-start(bf16[2048]{0:T(1024)(128)(2,1)} %param.16) | copy-start | bytes 12292
  41.5 4.3 copy-start
  41.5 4.6 copy-start.11
  41.5 5.2 copy-start.10
  41.5 20.5 %all-to-all-start.2 = ((bf16[4,4,4,32,384]{4,3,1,2,0:T(8,128)(2,1)}), bf16[4,4,4,32,384]{4,3,1,2,0:T(8,128)(2,1)S(1)}, u32[]{:S(2)}, u32[]{:S(2)}) async-start(bf16[4,4,4,32,384]{4,3,1,2,0:T(8,128)(2,1)} %broadcast_in_dim.18), calls=%async_computation.2 | async-start | bytes 3145728 | tf_op jit(solution)/shard_map/all_to_all | solution.py:23
  62.3 1.8 copy-start.1
  64.1 1.0 copy-start.15
  64.1 0.9 copy-start.16
  64.2 1.8 copy-start.17
  70.6 9.8 %copy-start.4 = (f32[4,128]{1,0:T(4,128)}, f32[4,128]{1,0:T(4,128)S(1)}, u32[]{:S(2)}) copy-start(f32[4,128]{1,0:T(4,128)S(1)} %get-tuple-element.32) | copy-start | bytes 6148
  70.6 9.8 %copy-start.5 = (f32[4,128]{1,0:T(4,128)}, f32[4,128]{1,0:T(4,128)S(1)}, u32[]{:S(2)}) copy-start(f32[4,128]{1,0:T(4,128)S(1)} %get-tuple-element.31) | copy-start | bytes 6148
  84.4 7.2 %copy-start.13 = (f32[1,128]{1,0:T(1,128)S(1)}, f32[1,128]{1,0:T(1,128)}, u32[]{:S(2)}) copy-start(f32[1,128]{1,0:T(1,128)} %slice.595) | copy-start | bytes 1540
  84.4 7.3 %copy-start.12 = (f32[1,128]{1,0:T(1,128)S(1)}, f32[1,128]{1,0:T(1,128)}, u32[]{:S(2)}) copy-start(f32[1,128]{1,0:T(1,128)} %slice.594) | copy-start | bytes 1540
  89.3 2.3 copy-start.14
  92.4 15.0 %copy-start.7 = (bf16[2048]{0:T(1024)(128)(2,1)S(1)}, bf16[2048]{0:T(1024)(128)(2,1)}, u32[]{:S(2)}) copy-start(bf16[2048]{0:T(1024)(128)(2,1)} %param.25) | copy-start | bytes 12292
  92.4 15.0 %copy-start.8 = (bf16[2048]{0:T(1024)(128)(2,1)S(1)}, bf16[2048]{0:T(1024)(128)(2,1)}, u32[]{:S(2)}) copy-start(bf16[2048]{0:T(1024)(128)(2,1)} %param.26) | copy-start | bytes 12292
  92.4 15.0 %copy-start.2 = (bf16[1024,32]{0,1:T(8,128)(2,1)S(1)}, bf16[1024,32]{0,1:T(8,128)(2,1)}, u32[]{:S(2)}) copy-start(bf16[1024,32]{0,1:T(8,128)(2,1)} %param.28) | copy-start | bytes 196612
  92.5 15.0 %copy-start.3 = (bf16[32,1024]{1,0:T(8,128)(2,1)S(1)}, bf16[32,1024]{1,0:T(8,128)(2,1)}, u32[]{:S(2)}) copy-start(bf16[32,1024]{1,0:T(8,128)(2,1)} %param.27) | copy-start | bytes 196612
  103.4 12.9 %all-to-all-start.4 = ((bf16[4,32,2048]{2,1,0:T(8,128)(2,1)}), bf16[4,32,2048]{2,1,0:T(8,128)(2,1)S(1)}, u32[]{:S(2)}, u32[]{:S(2)}) async-start(bf16[4,32,2048]{2,1,0:T(8,128)(2,1)} %bitcast.17), calls=%async_computation.4 | async-start | bytes 1048576 | tf_op jit(solution)/shard_map/all_to_all | solution.py:44
  117.2 11.2 %all-to-all-start.7 = ((bf16[4,32,2048]{2,1,0:T(8,128)(2,1)}), bf16[4,32,2048]{2,1,0:T(8,128)(2,1)S(1)}, u32[]{:S(2)}, u32[]{:S(2)}) async-start(bf16[4,32,2048]{2,1,0:T(8,128)(2,1)} %broadcast_in_dim.41), calls=%async_computation.7 | async-start | bytes 1048576 | tf_op jit(solution)/shard_map/all_to_all | solution.py:23
  519.7 17.3 %copy-start.9 = (bf16[2048]{0:T(1024)(128)(2,1)S(1)}, bf16[2048]{0:T(1024)(128)(2,1)}, u32[]{:S(2)}) copy-start(bf16[2048]{0:T(1024)(128)(2,1)} %param.29) | copy-start | bytes 12292
  533.5 12.6 %all-to-all-start.10 = ((bf16[4,32,2048]{2,1,0:T(8,128)(2,1)}), bf16[4,32,2048]{2,1,0:T(8,128)(2,1)S(1)}, u32[]{:S(2)}, u32[]{:S(2)}) async-start(bf16[4,32,2048]{2,1,0:T(8,128)(2,1)} %bitcast.23), calls=%async_computation.10 | async-start | bytes 1048576 | tf_op jit(solution)/shard_map/all_to_all | solution.py:44
